TPU v7x, 32 devices: a whole 2x2x4 slice. The times are simulated.
32 devices in a mesh: ep: 8 (over z, y), tp: 4 (over x, core).
Axes of the slice: x: 2, y: 2, z: 4, core: 2. Of those that a mesh axis runs over, the one named last changes fastest.
Arguments:
- mixer_input: bfloat16 [4096, 2048], P('ep'), may hold values from -6 to 6
- log_forget_total: float32 [16, 4096], P('tp'), may hold values from -684 to 0, as said below
- mixer_gain: float32 [2048], replicated, may hold values from 0.1 to 1.9
- w_query: bfloat16 [2048, 1024], P(None, 'tp'), may hold values from -1 to 1
- w_key: bfloat16 [2048, 256], P(None, 'tp'), may hold values from -8 to 8
- w_value: bfloat16 [2048, 256], P(None, 'tp'), may hold values from -0.125 to 0.125
- w_output: bfloat16 [1024, 2048], replicated, may hold values from -0.1875 to 0.1875
- mixer_post_gain: float32 [2048], replicated, may hold values from 0.1 to 1.9
- expert_input: bfloat16 [2048, 2048], P('ep'), may hold values from -6 to 6
- expert_ids: int32 [2048, 2], P('ep'), may hold values from 0 to 7, all different within a row; in each aligned block of 64 rows (0 to 63, 64 to 127, ...) at most 32 rows name the same one
- route_weight: float32 [2048, 2], P('ep'), may hold values from 0.1 to 1
- expert_gain: float32 [2048], replicated, may hold values from 0.1 to 1.9
- w_gate: bfloat16 [8, 2048, 3584], P('ep', None, 'tp'), may hold values from -0.125 to 0.125
- w_up: bfloat16 [8, 2048, 3584], P('ep', None, 'tp'), may hold values from -0.125 to 0.125
- w_down: bfloat16 [8, 3584, 2048], P('ep', 'tp'), may hold values from -0.09375 to 0.09375
- expert_post_gain: float32 [2048], replicated, may hold values from 0.1 to 1.9
Outputs:
- mixer_out: bfloat16 [4096, 2048], P(('ep', 'tp'))
- expert_out: bfloat16 [2048, 2048], P(('ep', 'tp'))
Inputs may be any that keep to these rules, and one draw needn't show every extreme that they name: `expert_ids`: in each aligned block of 64 tokens no expert is named by more than 32 of them. `log_forget_total`: each head's values never rise along the positions.
All inputs are finite; a program needn't handle non-finite values.
Results may differ from a plain program's by a relative error of at most 0.012.
The roundings to bfloat16 on the way count: a program that leaves them out, or rounds other values in their place, can miss the bound.
Values may be sent and summed in bfloat16 or wider, within the bound.
No kernel may reach another device: no remote copies, remote signals or barrier semaphores. Data moves between devices by JAX's collectives and lax.ppermute only.
A program may use at most 128 MiB of HBM per device.

v0:
```python
import math

import jax
import jax.numpy as jnp
from jax import lax
from jax.sharding import PartitionSpec as P

HD = 64
TOP_K = 2


NEG_FILL = -1e30
NORM_EPS = 1e-06


def norm_rows(values_in, gain_vec):
    widened = values_in.astype(jnp.float32)
    return (
        widened
        * lax.rsqrt(jnp.mean(widened * widened, axis=-1, keepdims=True) + NORM_EPS)
        * gain_vec
    )


def unchanged(present_state):
    return present_state


def mixer_half(
    mixer_input, log_forget_total, mixer_gain, w_query, w_key, w_value, w_output, mixer_post_gain
):
    row_count = mixer_input.shape[0]
    offset = lax.axis_index("ep") * row_count
    head_local = w_query.shape[1] // HD
    kv_local = w_key.shape[1] // HD
    group_size = head_local // kv_local
    normed = norm_rows(mixer_input, mixer_gain).astype(jnp.bfloat16)
    queries = (
        jnp.dot(normed, w_query, preferred_element_type=jnp.float32)
        .astype(jnp.bfloat16)
        .reshape(row_count, kv_local, group_size, HD)
    )
    key_rows = (
        jnp.dot(normed, w_key, preferred_element_type=jnp.float32)
        .astype(jnp.bfloat16)
        .reshape(row_count, kv_local, HD)
    )
    value_rows = (
        jnp.dot(normed, w_value, preferred_element_type=jnp.float32)
        .astype(jnp.bfloat16)
        .reshape(row_count, kv_local, HD)
    )
    gate_totals = log_forget_total.reshape(kv_local, group_size, -1)
    query_gate = lax.dynamic_slice_in_dim(gate_totals, offset, row_count, 2)
    query_pos = offset + jnp.arange(row_count, dtype=jnp.int32)
    last_row = offset + row_count - 1
    score_scale = HD ** (-0.5)
    start_state = (
        jnp.full((kv_local, group_size, row_count), NEG_FILL, jnp.float32),
        jnp.zeros((kv_local, group_size, row_count), jnp.float32),
        jnp.zeros((kv_local, group_size, row_count, HD), jnp.float32),
    )
    running = start_state
    key_piece = lax.all_gather(key_rows, "ep", axis=0, tiled=True)
    value_piece = lax.all_gather(value_rows, "ep", axis=0, tiled=True)
    piece_rows = key_piece.shape[0]
    block_rows = math.gcd(piece_rows, 512)
    block_total = piece_rows // block_rows
    key_blocks = key_piece.reshape(block_total, block_rows, kv_local, HD)
    value_blocks = value_piece.reshape(block_total, block_rows, kv_local, HD)

    def one_block(present_state, operands):
        key_block, value_block, block_index = operands
        block_first = block_index * block_rows

        def update(prior_value):
            row_max, denominator, numerator = prior_value
            key_gate = lax.dynamic_slice_in_dim(gate_totals, block_first, block_rows, 2)
            scores = (
                jnp.einsum("qgjd,kgd->gjqk", queries, key_block, preferred_element_type=jnp.float32)
                * score_scale
            )
            scores = scores + query_gate[:, :, :, None] - key_gate[:, :, None, :]
            visible = (block_first + jnp.arange(block_rows, dtype=jnp.int32))[None, :] <= query_pos[
                :, None
            ]
            scores = jnp.where(visible, scores, NEG_FILL)
            new_max = jnp.maximum(row_max, jnp.max(scores, axis=-1))
            shifted = jnp.where(visible, jnp.exp(scores - new_max[..., None]), 0.0)
            factor = jnp.exp(row_max - new_max)
            denominator = denominator * factor + jnp.sum(shifted, axis=-1)
            numerator = numerator * factor[..., None] + jnp.einsum(
                "gjqk,kgd->gjqd",
                shifted.astype(jnp.bfloat16),
                value_block,
                preferred_element_type=jnp.float32,
            )
            return (new_max, denominator, numerator)

        return (lax.cond(block_first <= last_row, update, unchanged, present_state), None)

    running, _ = lax.scan(
        one_block, running, (key_blocks, value_blocks, jnp.arange(block_total, dtype=jnp.int32))
    )
    row_max, denominator, numerator = running
    mixed_heads = (
        jnp.transpose(numerator / denominator[..., None], (2, 0, 1, 3))
        .reshape(row_count, head_local * HD)
        .astype(jnp.bfloat16)
    )
    by_rows = lax.all_to_all(mixed_heads, "tp", split_axis=0, concat_axis=1, tiled=True)
    projected = jnp.dot(by_rows, w_output, preferred_element_type=jnp.float32)
    return norm_rows(projected, mixer_post_gain).astype(jnp.bfloat16)


def expert_half(
    expert_input, expert_ids, route_weight, expert_gain, w_gate, w_up, w_down, expert_post_gain
):
    row_count = expert_input.shape[0]
    quarters = lax.axis_size("tp")
    experts = lax.axis_size("ep")
    quarter_rows = row_count // quarters
    slot_count = 2 * TOP_K * quarter_rows // experts
    own_quarter = lax.axis_index("tp")
    normed = norm_rows(expert_input, expert_gain).astype(jnp.bfloat16)
    padded_rows = jnp.concatenate([normed, jnp.zeros((1, normed.shape[1]), jnp.bfloat16)], axis=0)
    routed = expert_ids.reshape(quarters, quarter_rows * TOP_K)
    matches = (routed[:, :, None] == jnp.arange(experts, dtype=jnp.int32)[None, None, :]).astype(
        jnp.int32
    )
    slot_ranks = jnp.sum(jnp.cumsum(matches, axis=1) * matches, axis=2) - 1
    owners = (jnp.arange(row_count * TOP_K, dtype=jnp.int32) // TOP_K).reshape(
        quarters, quarter_rows * TOP_K
    )
    quarter_index = jnp.broadcast_to(jnp.arange(quarters, dtype=jnp.int32)[:, None], routed.shape)
    slot_table = (
        jnp.full((quarters, slot_count, experts), row_count, jnp.int32)
        .at[quarter_index, slot_ranks, routed]
        .set(owners)
    )
    gate_local = w_gate[0]
    up_local = w_up[0]
    down_local = w_down[0]
    unit_count = gate_local.shape[1]
    own_table = lax.dynamic_index_in_dim(slot_table, own_quarter, 0, keepdims=False)
    outgoing = padded_rows[own_table]
    arrived = lax.all_to_all(outgoing, "ep", split_axis=1, concat_axis=1, tiled=True)
    slot_rows = lax.all_gather(arrived[None], "tp", axis=0, tiled=True)
    flat_rows = slot_rows.reshape(-1, slot_rows.shape[-1])
    gate_part = jnp.dot(flat_rows, gate_local, preferred_element_type=jnp.float32)
    up_part = jnp.dot(flat_rows, up_local, preferred_element_type=jnp.float32)
    hidden = (
        (jax.nn.silu(gate_part) * up_part)
        .astype(jnp.bfloat16)
        .reshape(slot_rows.shape[:-1] + (unit_count,))
    )
    product = jnp.dot(
        hidden.reshape(-1, unit_count), down_local, preferred_element_type=jnp.float32
    )
    summed = lax.psum_scatter(
        product.reshape(lax.axis_size("tp") * 1, slot_count, experts, product.shape[-1]).astype(
            jnp.bfloat16
        ),
        "tp",
        scatter_dimension=0,
        tiled=True,
    ).astype(jnp.float32)
    results = summed[0].astype(jnp.bfloat16)
    returned = lax.all_to_all(results, "ep", split_axis=1, concat_axis=1, tiled=True)
    flat_results = returned.reshape(slot_count * experts, returned.shape[-1])
    own_routes = lax.dynamic_index_in_dim(routed, own_quarter, 0, keepdims=False)
    own_ranks = lax.dynamic_index_in_dim(slot_ranks, own_quarter, 0, keepdims=False)
    picked = flat_results[own_ranks * experts + own_routes].reshape(quarter_rows, TOP_K, -1)
    own_weights = lax.dynamic_slice_in_dim(
        route_weight, own_quarter * quarter_rows, quarter_rows, 0
    )
    combined = jnp.sum(own_weights[:, :, None] * picked.astype(jnp.float32), axis=1)
    return norm_rows(combined, expert_post_gain).astype(jnp.bfloat16)


def per_device(
    mixer_input,
    log_forget_total,
    mixer_gain,
    w_query,
    w_key,
    w_value,
    w_output,
    mixer_post_gain,
    expert_input,
    expert_ids,
    route_weight,
    expert_gain,
    w_gate,
    w_up,
    w_down,
    expert_post_gain,
):
    mixer_out = mixer_half(
        mixer_input,
        log_forget_total,
        mixer_gain,
        w_query,
        w_key,
        w_value,
        w_output,
        mixer_post_gain,
    )
    expert_out = expert_half(
        expert_input, expert_ids, route_weight, expert_gain, w_gate, w_up, w_down, expert_post_gain
    )
    return (mixer_out, expert_out)


def solution(mesh):
    placed = (
        P("ep", None),
        P("tp", None),
        P(),
        P(None, "tp"),
        P(None, "tp"),
        P(None, "tp"),
        P(),
        P(),
        P("ep", None),
        P("ep", None),
        P("ep", None),
        P(),
        P("ep", None, "tp"),
        P("ep", None, "tp"),
        P("ep", "tp", None),
        P(),
    )
    return jax.shard_map(
        per_device,
        mesh=mesh,
        in_specs=placed,
        out_specs=(P(("ep", "tp"), None), P(("ep", "tp"), None)),
        check_vma=False,
    )
```

profile of v0, /device:TPU:0, one launch (start us, length us, event | category | flops | bytes accessed | tf_op | source)
XLA Modules:
  0.0 324.2 jit_solution(3863174267052389493)
XLA Ops:
  7.2 0.9 copy.41
  9.2 29.5 %scatter_fusion = s32[4,32,8]{1,2,0:T(8,128)S(1)} fusion(s32[4,32,8]{1,2,0:T(8,128)S(1)} %broadcast_in_dim.39, s32[512]{0:T(512)S(1)} %fusion.52, s32[512]{0:T(512)S(1)} %fusion.54), kind=kCustom, calls=%fused_computation.2 | custom fusion | bytes 12288 | tf_op jit(solution)/shard_map/scatter | solution.py:139
  39.7 1.4 gather_fusion
  41.0 0.6 copy.44
  41.6 32.9 %all_to_all.26 = bf16[32,8,2048]{2,0,1:T(8,128)(2,1)S(1)} all-to-all(bf16[32,8,2048]{2,0,1:T(8,128)(2,1)S(1)} %copy.44), channel_id=1, replica_groups=mesh['ep'=8,'tp'=4] {'ep'}, dimensions={1} | all-to-all | bytes 2097152 | tf_op jit(solution)/shard_map/all_to_all | solution.py:147
  74.5 1.6 copy.45
  76.3 33.4 %all-gather.5.cloned.1.call-done = bf16[128,8,2048]{2,1,0:T(8,128)(2,1)} async-done(((bf16[32,8,2048]{2,1,0:T(8,128)(2,1)}), bf16[128,8,2048]{2,1,0:T(8,128)(2,1)}) %all-gather.5.cloned.1.call-update) | async-done | bytes 4194320 | tf_op jit(solution)/shard_map/all_gather | solution.py:148
  109.7 7.5 %fusion.32 = f32[1024,896]{1,0:T(8,128)S(1)} fusion(bf16[128,8,2048]{2,1,0:T(8,128)(2,1)} %all-gather.5.cloned.1.call-done, bf16[1,2048,896]{2,1,0:T(8,128)(2,1)} %param.33), kind=kOutput, calls=%fused_computation.40 | convolution fusion | flops 3758096384 | bytes 11534336 | tf_op jit(solution)/shard_map/dot_general | solution.py:151
  117.2 4.8 %multiply_convert_fusion = bf16[1024,896]{1,0:T(8,128)(2,1)S(1)} fusion(f32[1024,896]{1,0:T(8,128)S(1)} %fusion.32, bf16[1,2048,896]{2,1,0:T(8,128)(2,1)S(1)} %copy-done.11, bf16[128,8,2048]{2,1,0:T(8,128)(2,1)S(1)} %copy-done.10), kind=kOutput, calls=%fused_computation.48 | convolution fusion | flops 3763601408 | bytes 13369344 | tf_op jit(solution)/shard_map/dot_general | solution.py:150
  122.0 6.0 %convolution_convert_fusion = bf16[4,32,8,2048]{3,2,1,0:T(8,128)(2,1)} fusion(bf16[4,32,8,896]{3,2,1,0:T(8,128)(2,1)S(1)} %bitcast.163, bf16[1,896,2048]{2,1,0:T(8,128)(2,1)S(1)} %copy-done.12), kind=kOutput, calls=%fused_computation.44 | convolution fusion | flops 3760193536 | bytes 9699328 | tf_op jit(solution)/shard_map/dot_general | solution.py:157
  128.0 1.5 copy-done.1
  129.6 0.5 fusion.29
  130.1 2.2 fusion.31
  132.3 0.8 convolution_convert_fusion.3
  133.0 31.5 %all-gather = bf16[4096,64]{0,1:T(8,128)(2,1)S(1)} all-gather(bf16[512,64]{0,1:T(8,128)(2,1)S(1)} %convolution_convert_fusion.3), channel_id=2, replica_groups=mesh['ep'=8,'tp'=4] {'ep'}, dimensions={0}, use_global_device_ids=true | all-gather | bytes 589824 | tf_op jit(solution)/shard_map/all_gather | solution.py:64
  164.7 0.9 copy.37
  165.6 0.8 convolution_convert_fusion.2
  166.4 31.4 %all-gather.1 = bf16[4096,64]{0,1:T(8,128)(2,1)S(1)} all-gather(bf16[512,64]{0,1:T(8,128)(2,1)S(1)} %convolution_convert_fusion.2), channel_id=3, replica_groups=mesh['ep'=8,'tp'=4] {'ep'}, dimensions={0}, use_global_device_ids=true | all-gather | bytes 589824 | tf_op jit(solution)/shard_map/all_gather | solution.py:65
  198.0 1.0 copy.38
  199.0 0.7 dynamic-slice_bitcast_fusion.1
  199.7 1.5 convolution_convert_fusion.1
  201.2 18.1 %while.15 = (s32[]{:T(128)}, f32[1,4,512]{2,1,0:T(4,128)S(1)}, f32[1,4,512]{2,1,0:T(4,128)S(1)}, f32[1,4,512,64]{2,3,1,0:T(8,128)S(1)}, s32[8]{0:T(128)S(1)}, /*...) while((s32[]{:T(128)}, f32[1,4,512]{2,1,0:T(4,128)S(1)}, ...), condition=%wide.region_6.7_spmd.clone, body=%wide.region_1.6_spmd.clone.sunk | while | flops 288889856 | bytes 15283569 | solution.py:102
  201.2 0.7 dynamic_slice.79
  202.5 7.4 %conditional.3 = ((f32[1,4,512]{2,1,0:T(4,128)S(1)}, f32[1,4,512]{2,1,0:T(4,128)S(1)}, f32[1,4,512,64]{2,3,1,0:T(8,128)S(1)})) conditional(s32[]{:T(128)} %convert_element_type.123, (f32[1,4,512]{2,1,0:T(4,128)S(1)}, f32[1,4,512]{2,1,0:T(4,128)S(1)}, f32[1,4,512,64]{2,3,1,0:T(8,128)S(1)}) %tuple.48, (s32[]{:T(128)}, s32[]{:T(128)}, ...), branch_computations={%region_2.2_spmd, %region_3.5_spmd} | conditional | flops 288889856 | bytes 15281230 | solution.py:100
  202.5 0.8 dynamic-slice_bitcast_fusion
  203.6 2.2 fusion.6
  205.8 2.6 fusion.14
  208.4 1.5 fusion.5
  210.0 0.7 dynamic_slice.79
  211.3 0.7 dynamic_slice.79
  212.6 0.7 dynamic_slice.79
  214.0 0.7 dynamic_slice.79
  215.3 0.7 dynamic_slice.79
  216.7 0.7 dynamic_slice.79
  218.0 0.7 dynamic_slice.79
  219.5 0.7 copy.39
  220.2 3.4 %all-to-all-start = ((bf16[4,128,256]{1,2,0:T(8,128)(2,1)}), bf16[4,128,256]{1,2,0:T(8,128)(2,1)S(1)}, u32[]{:S(2)}, u32[]{:S(2)}) async-start(bf16[4,128,256]{1,2,0:T(8,128)(2,1)} %copy.39), calls=%async_computation | async-start | bytes 524288 | tf_op jit(solution)/shard_map/all_to_all | solution.py:111
  223.7 2.8 copy.46
  226.5 3.1 all-to-all-done
  229.6 57.5 %all-to-all-start.2 = ((bf16[32,8,2048]{2,0,1:T(8,128)(2,1)}), bf16[32,8,2048]{2,0,1:T(8,128)(2,1)S(1)}, u32[]{:S(2)}, u32[]{:S(2)}) async-start(bf16[32,8,2048]{2,0,1:T(8,128)(2,1)} %copy.46), calls=%async_computation.3 | async-start | bytes 2097152 | tf_op jit(solution)/shard_map/all_to_all | solution.py:169
  287.3 3.0 multiply_reduce_fusion.1
  290.3 1.0 multiply_convert_fusion.1
  291.3 21.4 %all-to-all-done.2 = bf16[32,8,2048]{2,0,1:T(8,128)(2,1)S(1)} async-done(((bf16[32,8,2048]{2,0,1:T(8,128)(2,1)}), bf16[32,8,2048]{2,0,1:T(8,128)(2,1)S(1)}, u32[]{:S(2)}, u32[]{:S(2)}) %all-to-all-start.2) | async-done | bytes 1048608 | tf_op jit(solution)/shard_map/all_to_all | solution.py:169
  312.7 0.6 copy.53
  313.3 0.9 gather_fusion.1
  314.2 0.7 reshape.287
  314.9 1.5 multiply_reduce_fusion
  316.6 0.8 multiply_convert_fusion.2
  (83 shorter events, 3.4 us)
Async XLA Ops:
  7.2 192.5 %copy-start = (bf16[2048,256]{1,0:T(8,128)(2,1)S(1)}, bf16[2048,256]{1,0:T(8,128)(2,1)}, u32[]{:S(2)}) copy-start(bf16[2048,256]{1,0:T(8,128)(2,1)} %param.23) | copy-start | bytes 3145732
  7.2 31.8 %copy-start.2 = (bf16[256,2048]{1,0:T(8,128)(2,1)S(1)}, bf16[256,2048]{1,0:T(8,128)(2,1)}, u32[]{:S(2)}) copy-start(bf16[256,2048]{1,0:T(8,128)(2,1)} %param.28) | copy-start | bytes 3145732
  7.2 32.1 %copy-start.5 = (f32[2048]{0:T(1024)S(1)}, f32[2048]{0:T(1024)}, u32[]{:S(2)}) copy-start(f32[2048]{0:T(1024)} %param.31) | copy-start | bytes 24580
  7.2 102.5 %all-gather.5.cloned.1.call-start = ((), (), s32[]{:S(2)}) async-start(), calls=%async_computation.5 | async-start | bytes 5242880 | tf_op jit(solution)/shard_map/all_gather | solution.py:148
  76.1 147.6 %reduce-scatter.2.cloned.1.call-start = ((), (), s32[]{:S(2)}) async-start(), calls=%async_computation.4 | async-start | bytes 5242880 | tf_op jit(solution)/shard_map/reduce_scatter | solution.py:160
  109.7 7.5 %copy-start.10 = (bf16[128,8,2048]{2,1,0:T(8,128)(2,1)S(1)}, bf16[128,8,2048]{2,1,0:T(8,128)(2,1)}, u32[]{:S(2)}) copy-start(bf16[128,8,2048]{2,1,0:T(8,128)(2,1)} %all-gather.5.cloned.1.call-done) | copy-start | bytes 12582916
  109.7 7.5 %copy-start.11 = (bf16[1,2048,896]{2,1,0:T(8,128)(2,1)S(1)}, bf16[1,2048,896]{2,1,0:T(8,128)(2,1)}, u32[]{:S(2)}) copy-start(bf16[1,2048,896]{2,1,0:T(8,128)(2,1)} %param.32) | copy-start | bytes 11010052
  117.2 4.8 %copy-start.12 = (bf16[1,896,2048]{2,1,0:T(8,128)(2,1)S(1)}, bf16[1,896,2048]{2,1,0:T(8,128)(2,1)}, u32[]{:S(2)}) copy-start(bf16[1,896,2048]{2,1,0:T(8,128)(2,1)} %param.34) | copy-start | bytes 11010052
  128.0 1.6 copy-start.1
  128.0 2.1 copy-start.6
  128.0 4.3 %copy-start.3 = (bf16[2048,64]{0,1:T(8,128)(2,1)S(1)}, bf16[2048,64]{0,1:T(8,128)(2,1)}, u32[]{:S(2)}) copy-start(bf16[2048,64]{0,1:T(8,128)(2,1)} %param.24) | copy-start | bytes 786436
  130.1 35.5 %copy-start.4 = (bf16[2048,64]{0,1:T(8,128)(2,1)S(1)}, bf16[2048,64]{0,1:T(8,128)(2,1)}, u32[]{:S(2)}) copy-start(bf16[2048,64]{0,1:T(8,128)(2,1)} %param.25) | copy-start | bytes 786436
  219.4 67.7 %copy-start.9 = (f32[256,2]{0,1:T(2,128)S(1)}, f32[256,2]{0,1:T(2,128)}, u32[]{:S(2)}) copy-start(f32[256,2]{0,1:T(2,128)} %param.30) | copy-start | bytes 6148
  220.2 9.4 %all-to-all-start = ((bf16[4,128,256]{1,2,0:T(8,128)(2,1)}), bf16[4,128,256]{1,2,0:T(8,128)(2,1)S(1)}, u32[]{:S(2)}, u32[]{:S(2)}) async-start(bf16[4,128,256]{1,2,0:T(8,128)(2,1)} %copy.39), calls=%async_computation | async-start | bytes 524288 | tf_op jit(solution)/shard_map/all_to_all | solution.py:111
  226.5 63.9 %copy-start.7 = (f32[2048]{0:T(1024)S(1)}, f32[2048]{0:T(1024)}, u32[]{:S(2)}) copy-start(f32[2048]{0:T(1024)} %param.27) | copy-start | bytes 24580
  229.6 83.1 %all-to-all-start.2 = ((bf16[32,8,2048]{2,0,1:T(8,128)(2,1)}), bf16[32,8,2048]{2,0,1:T(8,128)(2,1)S(1)}, u32[]{:S(2)}, u32[]{:S(2)}) async-start(bf16[32,8,2048]{2,0,1:T(8,128)(2,1)} %copy.46), calls=%async_computation.3 | async-start | bytes 2097152 | tf_op jit(solution)/shard_map/all_to_all | solution.py:169
  313.3 3.3 %copy-start.8 = (f32[2048]{0:T(1024)S(1)}, f32[2048]{0:T(1024)}, u32[]{:S(2)}) copy-start(f32[2048]{0:T(1024)} %param.35) | copy-start | bytes 24580
Sparse Core Ops, SparseCore 0:
  76.2 33.4 all-gather.4
  128.1 44.5 reduce-scatter.1
where the time goes:
time: 326 us; the launch traced here: 324 us
  blocking collectives  95.8 us (29%)
  starting transfers between devices  61.1 us (19%)
  waiting for transfers between devices  58 us (18%)
  local copies, waits for them, and re-layouts  51.1 us (16%)
  matrix products  29 us (9%)
  between operations  14.4 us (4%)
  other arithmetic  9.24 us (3%)
  loops' own time  5.57 us (2%)
    all_to_all x1, starting transfers between devices, expert_half(): lax.all_to_all(results, 'ep', split_axis=1, concat_axis=1, tiled=True)  57.5 us
    all_gather x1, waiting for transfers between devices, expert_half(): slot_rows = lax.all_gather(arrived[None], 'tp', axis=0, tiled=True)  33.4 us
    all_to_all x1, blocking collectives, expert_half(): lax.all_to_all(outgoing, 'ep', split_axis=1, concat_axis=1, tiled=True)  32.9 us
    all_gather x1, blocking collectives, mixer_half(): key_piece = lax.all_gather(key_rows, 'ep', axis=0, tiled=True)  31.5 us
    all_gather x1, blocking collectives, mixer_half(): value_piece = lax.all_gather(value_rows, 'ep', axis=0, tiled=True)  31.4 us
    scatter x1, local copies, waits for them, and re-layouts, expert_half(): slot_table = jnp.full((quarters, slot_count, experts), row_count, jnp.int...  29.5 us
    all_to_all x1, waiting for transfers between devices, expert_half(): lax.all_to_all(results, 'ep', split_axis=1, concat_axis=1, tiled=True)  21.4 us
    dot_general x1, matrix products, expert_half(): up_part = jnp.dot(flat_rows, up_local, preferred_element_type=jnp.float32)  7.49 us
  transfers between devices with their start and end apart: 4, of which 3 were waited for; matrix products, arithmetic and copies ran while one was open for 9% of the time, Pallas kernels for 0%

commit v1 on v0

v1 whole, which is shorter than its diff:
```python
import jax
import jax.numpy as jnp
from jax import lax
from jax.experimental import pallas as pl
from jax.experimental.pallas import tpu as pltpu
from jax.sharding import PartitionSpec as P

HD = 64
TOP_K = 2


NEG_FILL = -1e30
NORM_EPS = 1e-06


def norm_rows(values_in, gain_vec):
    widened = values_in.astype(jnp.float32)
    return (
        widened
        * lax.rsqrt(jnp.mean(widened * widened, axis=-1, keepdims=True) + NORM_EPS)
        * gain_vec
    )


def shift_pairs(count, step, wrap):
    return [(k, (k + step) % count) for k in range(count) if wrap or 0 <= k + step < count]


def flip(values_in, bit):
    count = lax.axis_size("tp")
    return lax.ppermute(values_in, "tp", [(k, k ^ bit) for k in range(count)])


def attention_kernel(rank_ref, query_ref, kv_ref, gate_ref, out_ref, wide_ref, max_ref, acc_ref):
    rows = query_ref.shape[0]
    heads = query_ref.shape[1] // HD
    kv_heads = kv_ref.shape[0]
    group = heads // kv_heads
    rank = rank_ref[0]
    low_half = lax.broadcasted_iota(jnp.int32, (rows, 2 * HD), 1) < HD
    for h in range(heads):
        one = query_ref[:, h * HD : (h + 1) * HD] * jnp.asarray(HD**-0.5, jnp.bfloat16)
        wide_ref[h] = jnp.concatenate([one, jnp.zeros_like(one)], axis=1)

    def scores_of(h, kv_block, gate_block):
        scores = lax.dot_general(
            wide_ref[h], kv_block, (((1,), (1,)), ((), ())), preferred_element_type=jnp.float32
        )
        return scores - gate_block[h : h + 1, :]

    def block(step, first):
        gate_block = gate_ref[rank - step]
        for g in range(kv_heads):
            kv_block = kv_ref[g, pl.ds(pl.multiple_of(step * rows, rows), rows), :]
            one_value = jnp.where(low_half, jnp.ones_like(kv_block), kv_block)
            for h in range(g * group, (g + 1) * group):
                scores = scores_of(h, kv_block, gate_block)
                if first:
                    visible = lax.broadcasted_iota(
                        jnp.int32, (rows, rows), 1
                    ) <= lax.broadcasted_iota(jnp.int32, (rows, rows), 0)
                    scores = jnp.where(visible, scores, NEG_FILL)
                    new_max = jnp.max(scores, axis=1, keepdims=True)
                else:
                    prior = max_ref[h][:, :1]
                    new_max = jnp.maximum(prior, jnp.max(scores, axis=1, keepdims=True))
                shifted = jnp.exp(scores - new_max).astype(jnp.bfloat16)
                term = jnp.dot(shifted, one_value, preferred_element_type=jnp.float32)
                if first:
                    acc_ref[h] = term
                else:
                    acc_ref[h] = acc_ref[h] * jnp.exp(prior - new_max) + term
                max_ref[h] = jnp.broadcast_to(new_max, (rows, 2 * HD))

    block(0, True)

    def loop_body(step, carry):
        block(step, False)
        return carry

    lax.fori_loop(1, rank + 1, loop_body, 0)
    for h in range(heads):
        total = acc_ref[h]
        out_ref[:, h * HD : (h + 1) * HD] = (total[:, HD:] / total[:, :HD]).astype(jnp.bfloat16)


def attend(rank, queries, kv_all, gates):
    rows = queries.shape[0]
    heads = queries.shape[1] // HD
    vmem = pl.BlockSpec(memory_space=pltpu.VMEM)
    return pl.pallas_call(
        attention_kernel,
        out_shape=jax.ShapeDtypeStruct(queries.shape, jnp.bfloat16),
        in_specs=[pl.BlockSpec(memory_space=pltpu.SMEM), vmem, vmem, vmem],
        out_specs=vmem,
        scratch_shapes=[
            pltpu.VMEM((heads, rows, 2 * HD), jnp.bfloat16),
            pltpu.VMEM((heads, rows, 2 * HD), jnp.float32),
            pltpu.VMEM((heads, rows, 2 * HD), jnp.float32),
        ],
        name="attend",
    )(rank.reshape(1), queries, kv_all, gates)


def mixer_start(mixer_input, log_forget_total, mixer_gain, w_query, w_key, w_value):
    row_count = mixer_input.shape[0]
    ranks = lax.axis_size("ep")
    head_local = w_query.shape[1] // HD
    kv_local = w_key.shape[1] // HD
    normed = norm_rows(mixer_input, mixer_gain).astype(jnp.bfloat16)
    key_rows = jnp.dot(normed, w_key, preferred_element_type=jnp.float32).astype(jnp.bfloat16)
    value_rows = jnp.dot(normed, w_value, preferred_element_type=jnp.float32).astype(jnp.bfloat16)
    own = jnp.concatenate(
        [
            key_rows.reshape(row_count, kv_local, HD),
            value_rows.reshape(row_count, kv_local, HD),
        ],
        axis=2,
    )
    own = jnp.transpose(own, (1, 0, 2))
    queries = jnp.dot(normed, w_query, preferred_element_type=jnp.float32).astype(jnp.bfloat16)
    gates = jnp.transpose(log_forget_total.reshape(head_local, ranks, row_count), (1, 0, 2))
    return own, queries, gates


def gather_kv(own):
    ranks = lax.axis_size("ep")
    pieces = [own]
    for step in range(1, ranks):
        pieces.append(lax.ppermute(own, "ep", shift_pairs(ranks, step, False)))
    return jnp.concatenate(pieces, axis=1)


def mixer_end(mixed_heads, w_output, mixer_post_gain):
    quarters = lax.axis_size("tp")
    mine = lax.axis_index("tp")
    rows = mixed_heads.shape[0] // quarters
    cut = mixed_heads.reshape(quarters, rows, mixed_heads.shape[1])
    pieces = []
    for bit in range(quarters):
        piece = lax.dynamic_index_in_dim(cut, mine ^ bit, 0, keepdims=False)
        pieces.append(flip(piece, bit) if bit else piece)
    stacked = jnp.stack(pieces)
    by_rows = jnp.concatenate(
        [
            lax.dynamic_index_in_dim(stacked, mine ^ source, 0, keepdims=False)
            for source in range(quarters)
        ],
        axis=1,
    )
    projected = jnp.dot(by_rows, w_output, preferred_element_type=jnp.float32)
    return norm_rows(projected, mixer_post_gain).astype(jnp.bfloat16)


def route(expert_input, expert_ids, route_weight, expert_gain):
    quarters = lax.axis_size("tp")
    experts = lax.axis_size("ep")
    quarter_rows = expert_input.shape[0] // quarters
    capacity = 2 * TOP_K * quarter_rows // experts
    first = lax.axis_index("tp") * quarter_rows
    own_rows = lax.dynamic_slice_in_dim(expert_input, first, quarter_rows, 0)
    own_ids = lax.dynamic_slice_in_dim(expert_ids, first, quarter_rows, 0)
    own_weight = lax.dynamic_slice_in_dim(route_weight, first, quarter_rows, 0)
    normed = norm_rows(own_rows, expert_gain).astype(jnp.bfloat16)
    named = (lax.axis_index("ep") + jnp.arange(experts, dtype=jnp.int32)) % experts
    chosen = own_ids[:, :, None] == named[None, None, :]
    matches = jnp.any(chosen, axis=1)
    weights = jnp.sum(jnp.where(chosen, own_weight[:, :, None], 0.0), axis=1)
    position = jnp.arange(quarter_rows, dtype=jnp.int32)
    before = (position[None, :] < position[:, None]).astype(jnp.bfloat16)
    ranks = jnp.dot(before, matches.astype(jnp.bfloat16), preferred_element_type=jnp.float32)
    ranks = jnp.where(matches, ranks.astype(jnp.int32), -1)
    placed = ranks[:, :, None] == jnp.arange(capacity, dtype=jnp.int32)[None, None, :]
    share = jnp.where(placed, weights[:, :, None], 0.0).reshape(quarter_rows, experts * capacity)
    placed = placed.reshape(quarter_rows, experts * capacity).astype(jnp.bfloat16)
    outgoing = lax.dot_general(
        placed, normed, (((0,), (0,)), ((), ())), preferred_element_type=jnp.float32
    ).astype(jnp.bfloat16)
    return outgoing, share, capacity


def exchange(rows, capacity, sign):
    experts = lax.axis_size("ep")
    pieces = [rows[:capacity]]
    for step in range(1, experts):
        piece = rows[step * capacity : (step + 1) * capacity]
        pieces.append(lax.ppermute(piece, "ep", shift_pairs(experts, sign * step, True)))
    return jnp.concatenate(pieces, axis=0)


def expert_rows_of(rows, gate_local, up_local, down_local):
    gate_part = jnp.dot(rows, gate_local, preferred_element_type=jnp.float32)
    up_part = jnp.dot(rows, up_local, preferred_element_type=jnp.float32)
    hidden = (jax.nn.silu(gate_part) * up_part).astype(jnp.bfloat16)
    return jnp.dot(hidden, down_local, preferred_element_type=jnp.float32).astype(jnp.bfloat16)


def combine(returned, share, expert_post_gain):
    high = lax.reduce_precision(share, 8, 7)
    low = lax.reduce_precision(share - high, 8, 7)
    combined = jnp.dot(
        high.astype(jnp.bfloat16), returned, preferred_element_type=jnp.float32
    ) + jnp.dot(low.astype(jnp.bfloat16), returned, preferred_element_type=jnp.float32)
    return norm_rows(combined, expert_post_gain).astype(jnp.bfloat16)


def per_device(
    mixer_input,
    log_forget_total,
    mixer_gain,
    w_query,
    w_key,
    w_value,
    w_output,
    mixer_post_gain,
    expert_input,
    expert_ids,
    route_weight,
    expert_gain,
    w_gate,
    w_up,
    w_down,
    expert_post_gain,
):
    outgoing, share, capacity = route(expert_input, expert_ids, route_weight, expert_gain)
    own_kv, queries, gates = mixer_start(
        mixer_input, log_forget_total, mixer_gain, w_query, w_key, w_value
    )
    arrived = exchange(outgoing, capacity, 1)
    kv_all = gather_kv(own_kv)
    bits = []
    bit = 1
    while bit < lax.axis_size("tp"):
        bits.append(bit)
        bit *= 2
    rows_of = {0: arrived}
    for bit in reversed(bits):
        for held in list(rows_of):
            rows_of[held | bit] = flip(rows_of[held], bit)
    mixed_heads = attend(lax.axis_index("ep"), queries, kv_all, gates)
    near = jnp.concatenate([rows_of[0], rows_of[1]], axis=0)
    far = jnp.concatenate([rows_of[2], rows_of[3]], axis=0)
    slots = arrived.shape[0]
    near_terms = expert_rows_of(near, w_gate[0], w_up[0], w_down[0])
    far_terms = expert_rows_of(far, w_gate[0], w_up[0], w_down[0])
    far_got = flip(far_terms[slots:], 1)
    near_got = flip(near_terms[slots:], 1)
    far_sum = far_terms[:slots].astype(jnp.float32) + far_got.astype(jnp.float32)
    crossed = flip(far_sum.astype(jnp.bfloat16), 2)
    near_sum = near_terms[:slots].astype(jnp.float32) + near_got.astype(jnp.float32)
    results = (near_sum + crossed.astype(jnp.float32)).astype(jnp.bfloat16)
    mixer_out = mixer_end(mixed_heads, w_output, mixer_post_gain)
    returned = exchange(results, capacity, -1)
    expert_out = combine(returned, share, expert_post_gain)
    return (mixer_out, expert_out)


def solution(mesh):
    placed = (
        P("ep", None),
        P("tp", None),
        P(),
        P(None, "tp"),
        P(None, "tp"),
        P(None, "tp"),
        P(),
        P(),
        P("ep", None),
        P("ep", None),
        P("ep", None),
        P(),
        P("ep", None, "tp"),
        P("ep", None, "tp"),
        P("ep", "tp", None),
        P(),
    )
    return jax.shard_map(
        per_device,
        mesh=mesh,
        in_specs=placed,
        out_specs=(P(("ep", "tp"), None), P(("ep", "tp"), None)),
        check_vma=False,
    )
```

time: 326 us -> 186 us (0.57)
  blocking collectives: 95.8 us -> 0 us
  local copies, waits for them, and re-layouts: 51.1 us -> 19.7 us
  between operations: 14.4 us -> 1.07 us
  waiting for transfers between devices: 58 us -> 47.2 us
  starting transfers between devices: 61.1 us -> 69.1 us
  matrix products: 29 us -> 34.8 us
  loops' own time: 5.57 us -> 0 us
  Pallas kernels: 0 us -> 4.37 us
    ppermute x0 -> x30, starting transfers between devices: none -> 69.1 us  [the longest x7 33.3 us: gather_kv(): pieces.append(lax.ppermute(own, 'ep', shift_pairs(ranks, step, False)))]
    all_gather x2 -> x0, blocking collectives: 62.9 us -> none  [the longest x1 31.5 us: mixer_half(): key_piece = lax.all_gather(key_rows, 'ep', axis=0, tiled=True)]
    all_to_all x2 -> x0, starting transfers between devices: 60.9 us -> none  [the longest x1 57.5 us: expert_half(): lax.all_to_all(results, 'ep', split_axis=1, concat_axis=1, tiled=True)]
    ppermute x0 -> x30, waiting for transfers between devices: none -> 47.2 us  [the longest x14 28.7 us: exchange(): lax.ppermute(piece, 'ep', shift_pairs(experts, sign * step, True))]
    all_gather x1 -> x0, waiting for transfers between devices: 33.4 us -> none  [expert_half(): slot_rows = lax.all_gather(arrived[None], 'tp', axis=0, tiled=True)]
    all_to_all x1 -> x0, blocking collectives: 32.9 us -> none  [expert_half(): lax.all_to_all(outgoing, 'ep', split_axis=1, concat_axis=1, tiled=True)]
    scatter x1 -> x0, local copies, waits for them, and re-layouts: 29.5 us -> none  [expert_half(): slot_table = jnp.full((quarters, slot_count, experts), row_count, jnp.int...]
    all_to_all x2 -> x0, waiting for transfers between devices: 24.5 us -> none  [the longest x1 21.4 us: expert_half(): lax.all_to_all(results, 'ep', split_axis=1, concat_axis=1, tiled=True)]
  transfers between devices with their start and end apart: 4 -> 30, of which waited for: 3 -> 9; matrix products, arithmetic and copies ran while one was open for 9% -> 29% of each run, Pallas kernels for 0% -> 2%
where the time goes in v1:
time: 186 us; the launch traced here: 185 us
  starting transfers between devices  69.1 us (37%)
  waiting for transfers between devices  47.2 us (25%)
  matrix products  34.8 us (19%)
  local copies, waits for them, and re-layouts  19.7 us (11%)
  other arithmetic  8.95 us (5%)
  Pallas kernels  4.37 us (2%)
    ppermute x7, starting transfers between devices, gather_kv(): pieces.append(lax.ppermute(own, 'ep', shift_pairs(ranks, step, False)))  33.3 us
    ppermute x14, starting transfers between devices, exchange(): lax.ppermute(piece, 'ep', shift_pairs(experts, sign * step, True))  31.1 us
    ppermute x14, waiting for transfers between devices, exchange(): lax.ppermute(piece, 'ep', shift_pairs(experts, sign * step, True))  28.7 us
    dot_general x2, matrix products, expert_rows_of(): jnp.dot(hidden, down_local, preferred_element_type=jnp.float32)  19.1 us
    ppermute x9, waiting for transfers between devices, flip(): return lax.ppermute(values_in, 'tp', [(k, k ^ bit) for k in range(count)])  18.5 us
    unnamed x53, local copies, waits for them, and re-layouts  13.2 us
    dot_general x2, matrix products, expert_rows_of(): up_part = jnp.dot(rows, up_local, preferred_element_type=jnp.float32)  7.24 us
    ppermute x9, starting transfers between devices, flip(): return lax.ppermute(values_in, 'tp', [(k, k ^ bit) for k in range(count)])  4.75 us
  transfers between devices with their start and end apart: 30, of which 9 were waited for; matrix products, arithmetic and copies ran while one was open for 29% of the time, Pallas kernels for 2%

profile of v1, /device:TPU:0, one launch (start us, length us, event | category | flops | bytes accessed | tf_op | source)
XLA Modules:
  0.0 185.3 jit_solution(424331046716139340)
XLA Ops:
  0.7 0.9 constant_dynamic-slice_fusion.1
  1.9 1.1 fusion.34
  3.1 1.5 convolution_convert_fusion
  5.4 3.0 %collective-permute-start.10 = (bf16[32,2048]{1,0:T(8,128)(2,1)S(1)}, bf16[32,2048]{1,0:T(8,128)(2,1)S(1)}, u32[]{:S(2)}, u32[]{:S(2)}) collective-permute-start(bf16[32,2048]{1,0:T(8,128)(2,1)S(1)} %get-tuple-element.19), channel_id=1, source_target_pairs={{0,4},{4,8},{8,12},{12,16},{16,20},{20,24},{24,28},{28,0},{1,5},{5... | collective-permute-start | bytes 393224 | tf_op jit(solution)/shard_map/ppermute | solution.py:187
  8.9 0.8 fusion.21
  9.9 0.8 fusion.22
  10.6 0.8 constant_dynamic-update-slice_fusion.7
  11.4 3.4 %collective-permute-start = (bf16[1,512,128]{2,1,0:T(8,128)(2,1)}, bf16[1,512,128]{2,1,0:T(8,128)(2,1)S(1)}, u32[]{:S(2)}, u32[]{:S(2)}) collective-permute-start(bf16[1,512,128]{2,1,0:T(8,128)(2,1)} %get-tuple-element.3), channel_id=1, source_target_pairs={{0,4},{4,8},{8,12},{12,16},{16,20},{20,24},{24,28},{1,5},{5,9},{9,... | collective-permute-start | bytes 393224 | tf_op jit(solution)/shard_map/ppermute | solution.py:130
  14.9 3.5 %collective-permute-start.1 = (bf16[1,512,128]{2,1,0:T(8,128)(2,1)}, bf16[1,512,128]{2,1,0:T(8,128)(2,1)S(1)}, u32[]{:S(2)}, u32[]{:S(2)}) collective-permute-start(bf16[1,512,128]{2,1,0:T(8,128)(2,1)} %get-tuple-element.3), channel_id=1, source_target_pairs={{0,8},{4,12},{8,16},{12,20},{16,24},{20,28},{1,9},{5,13},{9,17},{1... | collective-permute-start | bytes 393224 | tf_op jit(solution)/shard_map/ppermute | solution.py:130
  18.3 4.5 %collective-permute-start.2 = (bf16[1,512,128]{2,1,0:T(8,128)(2,1)}, bf16[1,512,128]{2,1,0:T(8,128)(2,1)S(1)}, u32[]{:S(2)}, u32[]{:S(2)}) collective-permute-start(bf16[1,512,128]{2,1,0:T(8,128)(2,1)} %get-tuple-element.3), channel_id=1, source_target_pairs={{0,12},{4,16},{8,20},{12,24},{16,28},{1,13},{5,17},{9,21},{13,25},... | collective-permute-start | bytes 393224 | tf_op jit(solution)/shard_map/ppermute | solution.py:130
  23.6 6.5 %collective-permute-done.11 = bf16[32,2048]{1,0:T(8,128)(2,1)S(1)} collective-permute-done((bf16[32,2048]{1,0:T(8,128)(2,1)S(1)}, bf16[32,2048]{1,0:T(8,128)(2,1)S(1)}, u32[]{:S(2)}, u32[]{:S(2)}) %collective-permute-start.11) | collective-permute-done | bytes 131104 | tf_op jit(solution)/shard_map/ppermute | solution.py:187
  30.2 1.4 collective-permute-start.13
  32.3 1.8 collective-permute-done.12
  34.1 4.5 %collective-permute-start.14 = (bf16[32,2048]{1,0:T(8,128)(2,1)S(1)}, bf16[32,2048]{1,0:T(8,128)(2,1)S(1)}, u32[]{:S(2)}, u32[]{:S(2)}) collective-permute-start(bf16[32,2048]{1,0:T(8,128)(2,1)S(1)} %get-tuple-element.15), channel_id=1, source_target_pairs={{0,20},{4,24},{8,28},{12,0},{16,4},{20,8},{24,12},{28,16},{1,21},{... | collective-permute-start | bytes 393224 | tf_op jit(solution)/shard_map/ppermute | solution.py:187
  39.2 4.4 %collective-permute-start.15 = (bf16[32,2048]{1,0:T(8,128)(2,1)S(1)}, bf16[32,2048]{1,0:T(8,128)(2,1)S(1)}, u32[]{:S(2)}, u32[]{:S(2)}) collective-permute-start(bf16[32,2048]{1,0:T(8,128)(2,1)S(1)} %get-tuple-element.14), channel_id=1, source_target_pairs={{0,24},{4,28},{8,0},{12,4},{16,8},{20,12},{24,16},{28,20},{1,25},{... | collective-permute-start | bytes 393224 | tf_op jit(solution)/shard_map/ppermute | solution.py:187
  44.7 3.8 %collective-permute-start.16 = (bf16[32,2048]{1,0:T(8,128)(2,1)S(1)}, bf16[32,2048]{1,0:T(8,128)(2,1)S(1)}, u32[]{:S(2)}, u32[]{:S(2)}) collective-permute-start(bf16[32,2048]{1,0:T(8,128)(2,1)S(1)} %get-tuple-element.13), channel_id=1, source_target_pairs={{0,28},{4,0},{8,4},{12,8},{16,12},{20,16},{24,20},{28,24},{1,29},{... | collective-permute-start | bytes 393224 | tf_op jit(solution)/shard_map/ppermute | solution.py:187
  49.9 1.7 collective-permute-done.16
  52.3 1.5 collective-permute-start.19
  53.8 1.5 convolution_convert_fusion.1.query_ref
  55.3 2.0 %collective-permute-start.3 = (bf16[1,512,128]{2,1,0:T(8,128)(2,1)}, bf16[1,512,128]{2,1,0:T(8,128)(2,1)S(1)}, u32[]{:S(2)}, u32[]{:S(2)}) collective-permute-start(bf16[1,512,128]{2,1,0:T(8,128)(2,1)} %get-tuple-element.3), channel_id=1, source_target_pairs={{0,16},{4,20},{8,24},{12,28},{1,17},{5,21},{9,25},{13,29},{2,18},{... | collective-permute-start | bytes 393224 | tf_op jit(solution)/shard_map/ppermute | solution.py:130
  58.0 4.9 %collective-permute-start.4 = (bf16[1,512,128]{2,1,0:T(8,128)(2,1)}, bf16[1,512,128]{2,1,0:T(8,128)(2,1)S(1)}, u32[]{:S(2)}, u32[]{:S(2)}) collective-permute-start(bf16[1,512,128]{2,1,0:T(8,128)(2,1)} %get-tuple-element.3), channel_id=1, source_target_pairs={{0,20},{4,24},{8,28},{1,21},{5,25},{9,29},{2,22},{6,26},{10,30},{3... | collective-permute-start | bytes 393224 | tf_op jit(solution)/shard_map/ppermute | solution.py:130
  63.6 1.8 collective-permute-start.5
  66.1 13.3 %collective-permute-start.6 = (bf16[1,512,128]{2,1,0:T(8,128)(2,1)}, bf16[1,512,128]{2,1,0:T(8,128)(2,1)S(1)}, u32[]{:S(2)}, u32[]{:S(2)}) collective-permute-start(bf16[1,512,128]{2,1,0:T(8,128)(2,1)} %get-tuple-element.3), channel_id=1, source_target_pairs={{0,28},{1,29},{2,30},{3,31}} | collective-permute-start | bytes 393224 | tf_op jit(solution)/shard_map/ppermute | solution.py:130
  81.3 1.4 constant_dynamic-update-slice_fusion.24
  82.9 0.8 copy-done.12
  83.7 3.6 %fusion.9 = f32[512,896]{1,0:T(8,128)} fusion(bf16[512,2048]{1,0:T(8,128)(2,1)S(1)} %constant_dynamic-update-slice_fusion.15, bf16[1,2048,896]{2,1,0:T(8,128)(2,1)S(1)} %copy-done.12), kind=kOutput, calls=%fused_computation.11 | convolution fusion | flops 1879048192 | bytes 7602176 | tf_op jit(solution)/shard_map/dot_general | solution.py:193
  87.4 1.3 copy-done.3
  88.7 3.7 %fusion.7 = f32[512,896]{1,0:T(8,128)} fusion(bf16[512,2048]{1,0:T(8,128)(2,1)S(1)} %constant_dynamic-update-slice_fusion.23, bf16[1,2048,896]{2,1,0:T(8,128)(2,1)S(1)} %copy-done.12), kind=kOutput, calls=%fused_computation.9 | convolution fusion | flops 1879048192 | bytes 7602176 | tf_op jit(solution)/shard_map/dot_general | solution.py:193
  92.3 8.9 %fusion.18 = bf16[512,2048]{1,0:T(8,128)(2,1)S(1)} fusion(bf16[1,896,2048]{2,1,0:T(8,128)(2,1)} %param.30, f32[512,896]{1,0:T(8,128)} %fusion.7, bf16[512,2048]{1,0:T(8,128)(2,1)} %copy-done.3, bf16[1,2048,896]{2,1,0:T(8,128)(2,1)} %param.28), kind=kOutput, calls=%fused_computation.18 | convolution fusion | flops 3761897472 | bytes 13369344 | tf_op jit(solution)/shard_map/dot_general | solution.py:195
  101.2 1.1 slice.91
  102.4 10.2 %fusion.15 = bf16[512,2048]{1,0:T(8,128)(2,1)} fusion(bf16[1,896,2048]{2,1,0:T(8,128)(2,1)} %param.30, f32[512,896]{1,0:T(8,128)} %fusion.9, bf16[512,2048]{1,0:T(8,128)(2,1)} %copy-done.8, bf16[1,2048,896]{2,1,0:T(8,128)(2,1)} %param.28), kind=kOutput, calls=%fused_computation.17 | convolution fusion | flops 3761897472 | bytes 13369344 | tf_op jit(solution)/shard_map/dot_general | solution.py:195
  112.6 2.3 %slice.89 = bf16[256,2048]{1,0:T(8,128)(2,1)} slice(bf16[512,2048]{1,0:T(8,128)(2,1)} %fusion.15), slice={[256:512], [0:2048]} | slice | bytes 2097152 | tf_op jit(solution)/shard_map/slice | solution.py:247
  115.4 2.6 %add_convert_fusion.1 = bf16[256,2048]{1,0:T(8,128)(2,1)} fusion(bf16[256,2048]{1,0:T(8,128)(2,1)} %collective-permute-done.21, bf16[512,2048]{1,0:T(8,128)(2,1)S(1)} %fusion.18), kind=kLoop, calls=%fused_computation.22 | loop fusion | flops 2097152 | bytes 3145728 | tf_op jit(solution)/shard_map/convert_element_type | solution.py:249
  119.2 4.4 %attend.1 = bf16[512,256]{1,0:T(8,128)(2,1)} custom-call(s32[1]{0:T(128)} %bitcast.rank_ref, bf16[512,256]{1,0:T(8,128)(2,1)} %convolution_convert_fusion.1.query_ref, bf16[1,4096,128]{2,1,0:T(8,128)(2,1)} %constant_dynamic-update-slice_fusion.kv_ref, f32[8,4,512]{2,1,0:T(4,128)} %bitcast.83), custom_call_target="tpu_custom_call" | custom-call | tf_op jit(solution)/shard_map/attend/pallas_call | solution.py:91
  123.6 1.0 constant_dynamic-slice_fusion.2
  124.6 1.5 collective-permute-start.8
  127.0 18.5 %collective-permute-done.8 = bf16[128,256]{1,0:T(8,128)(2,1)S(1)} collective-permute-done((bf16[128,256]{1,0:T(8,128)(2,1)S(1)}, bf16[128,256]{1,0:T(8,128)(2,1)S(1)}, u32[]{:S(2)}, u32[]{:S(2)}) %collective-permute-start.8) | collective-permute-done | bytes 65568 | tf_op jit(solution)/shard_map/ppermute | solution.py:31
  145.5 3.2 %multiply_reduce_fusion = (f32[128]{0:T(128)S(1)}, f32[128,2048]{1,0:T(8,128)S(1)}) fusion(bf16[1024,2048]{1,0:T(8,128)(2,1)} %param.22, bf16[128,256]{1,0:T(8,128)(2,1)S(1)} %get-tuple-element.22, bf16[128,256]{1,0:T(8,128)(2,1)S(1)} %get-tuple-element.23, bf16[128,256]{1,0:T(8,128)(2,1)S(1)} %get-tuple-element.24, bf16[128,256]{1,0:T(8,128)(2,1)S(1)} %get-tuple-element.21), kind=kOutput, calls=%fused_computation.33 | convolution fusion | flops 538443648 | bytes 5505536 | tf_op jit(solution)/shard_map/dot_general | solution.py:151
  148.7 1.7 add_convert_fusion
  150.6 8.1 %collective-permute-start.23 = (bf16[32,2048]{1,0:T(8,128)(2,1)S(1)}, bf16[32,2048]{1,0:T(8,128)(2,1)S(1)}, u32[]{:S(2)}, u32[]{:S(2)}) collective-permute-start(bf16[32,2048]{1,0:T(8,128)(2,1)S(1)} %get-tuple-element.10), channel_id=1, source_target_pairs={{0,28},{4,0},{8,4},{12,8},{16,12},{20,16},{24,20},{28,24},{1,29},{... | collective-permute-start | bytes 393224 | tf_op jit(solution)/shard_map/ppermute | solution.py:187
  158.7 0.9 multiply_convert_fusion.2
  159.6 3.4 %collective-permute-start.26 = (bf16[32,2048]{1,0:T(8,128)(2,1)S(1)}, bf16[32,2048]{1,0:T(8,128)(2,1)S(1)}, u32[]{:S(2)}, u32[]{:S(2)}) collective-permute-start(bf16[32,2048]{1,0:T(8,128)(2,1)S(1)} %get-tuple-element.7), channel_id=1, source_target_pairs={{0,16},{4,20},{8,24},{12,28},{16,0},{20,4},{24,8},{28,12},{1,17},{... | collective-permute-start | bytes 393224 | tf_op jit(solution)/shard_map/ppermute | solution.py:187
  163.1 1.5 collective-permute-start.28
  164.6 0.8 collective-permute-done.24
  166.1 2.1 %collective-permute-done.25 = bf16[32,2048]{1,0:T(8,128)(2,1)S(1)} collective-permute-done((bf16[32,2048]{1,0:T(8,128)(2,1)S(1)}, bf16[32,2048]{1,0:T(8,128)(2,1)S(1)}, u32[]{:S(2)}, u32[]{:S(2)}) %collective-permute-start.25) | collective-permute-done | bytes 131104 | tf_op jit(solution)/shard_map/ppermute | solution.py:187
  168.3 9.1 %collective-permute-done.26 = bf16[32,2048]{1,0:T(8,128)(2,1)S(1)} collective-permute-done((bf16[32,2048]{1,0:T(8,128)(2,1)S(1)}, bf16[32,2048]{1,0:T(8,128)(2,1)S(1)}, u32[]{:S(2)}, u32[]{:S(2)}) %collective-permute-start.26) | collective-permute-done | bytes 131104 | tf_op jit(solution)/shard_map/ppermute | solution.py:187
  177.4 6.2 %collective-permute-done.27 = bf16[32,2048]{1,0:T(8,128)(2,1)S(1)} collective-permute-done((bf16[32,2048]{1,0:T(8,128)(2,1)S(1)}, bf16[32,2048]{1,0:T(8,128)(2,1)S(1)}, u32[]{:S(2)}, u32[]{:S(2)}) %collective-permute-start.27) | collective-permute-done | bytes 131104 | tf_op jit(solution)/shard_map/ppermute | solution.py:187
  184.4 0.8 multiply_convert_fusion.5
  (108 shorter events, 15.6 us)
Async XLA Ops:
  0.6 53.1 %copy-start = (bf16[2048,256]{1,0:T(8,128)(2,1)S(1)}, bf16[2048,256]{1,0:T(8,128)(2,1)}, u32[]{:S(2)}) copy-start(bf16[2048,256]{1,0:T(8,128)(2,1)} %param.19) | copy-start | bytes 3145732
  0.6 7.7 %copy-start.1 = (bf16[512,2048]{1,0:T(8,128)(2,1)S(1)}, bf16[512,2048]{1,0:T(8,128)(2,1)}, u32[]{:S(2)}) copy-start(bf16[512,2048]{1,0:T(8,128)(2,1)} %param.16) | copy-start | bytes 6291460
  0.7 1.0 copy-start.9
  4.6 4.3 %copy-start.13 = (bf16[2048,64]{0,1:T(8,128)(2,1)S(1)}, bf16[2048,64]{0,1:T(8,128)(2,1)}, u32[]{:S(2)}) copy-start(bf16[2048,64]{0,1:T(8,128)(2,1)} %param.20) | copy-start | bytes 786436
  4.6 4.3 %copy-start.15 = (f32[2048]{0:T(1024)S(1)}, f32[2048]{0:T(1024)}, u32[]{:S(2)}) copy-start(f32[2048]{0:T(1024)} %param.18) | copy-start | bytes 24580
  5.4 17.5 %collective-permute-start.10 = (bf16[32,2048]{1,0:T(8,128)(2,1)S(1)}, bf16[32,2048]{1,0:T(8,128)(2,1)S(1)}, u32[]{:S(2)}, u32[]{:S(2)}) collective-permute-start(bf16[32,2048]{1,0:T(8,128)(2,1)S(1)} %get-tuple-element.19), channel_id=1, source_target_pairs={{0,4},{4,8},{8,12},{12,16},{16,20},{20,24},{24,28},{28,0},{1,5},{5... | collective-permute-start | bytes 393224 | tf_op jit(solution)/shard_map/ppermute | solution.py:187
  8.9 1.0 copy-start.14
  11.4 43.9 %collective-permute-start = (bf16[1,512,128]{2,1,0:T(8,128)(2,1)}, bf16[1,512,128]{2,1,0:T(8,128)(2,1)S(1)}, u32[]{:S(2)}, u32[]{:S(2)}) collective-permute-start(bf16[1,512,128]{2,1,0:T(8,128)(2,1)} %get-tuple-element.3), channel_id=1, source_target_pairs={{0,4},{4,8},{8,12},{12,16},{16,20},{20,24},{24,28},{1,5},{5,9},{9,... | collective-permute-start | bytes 393224 | tf_op jit(solution)/shard_map/ppermute | solution.py:130
  14.9 43.1 %collective-permute-start.1 = (bf16[1,512,128]{2,1,0:T(8,128)(2,1)}, bf16[1,512,128]{2,1,0:T(8,128)(2,1)S(1)}, u32[]{:S(2)}, u32[]{:S(2)}) collective-permute-start(bf16[1,512,128]{2,1,0:T(8,128)(2,1)} %get-tuple-element.3), channel_id=1, source_target_pairs={{0,8},{4,12},{8,16},{12,20},{16,24},{20,28},{1,9},{5,13},{9,17},{1... | collective-permute-start | bytes 393224 | tf_op jit(solution)/shard_map/ppermute | solution.py:130
  18.3 45.2 %collective-permute-start.2 = (bf16[1,512,128]{2,1,0:T(8,128)(2,1)}, bf16[1,512,128]{2,1,0:T(8,128)(2,1)S(1)}, u32[]{:S(2)}, u32[]{:S(2)}) collective-permute-start(bf16[1,512,128]{2,1,0:T(8,128)(2,1)} %get-tuple-element.3), channel_id=1, source_target_pairs={{0,12},{4,16},{8,20},{12,24},{16,28},{1,13},{5,17},{9,21},{13,25},... | collective-permute-start | bytes 393224 | tf_op jit(solution)/shard_map/ppermute | solution.py:130
  22.8 7.4 %collective-permute-start.11 = (bf16[32,2048]{1,0:T(8,128)(2,1)S(1)}, bf16[32,2048]{1,0:T(8,128)(2,1)S(1)}, u32[]{:S(2)}, u32[]{:S(2)}) collective-permute-start(bf16[32,2048]{1,0:T(8,128)(2,1)S(1)} %get-tuple-element.18), channel_id=1, source_target_pairs={{0,8},{4,12},{8,16},{12,20},{16,24},{20,28},{24,0},{28,4},{1,9},{5... | collective-permute-start | bytes 393224 | tf_op jit(solution)/shard_map/ppermute | solution.py:187
  22.9 11.2 %collective-permute-start.12 = (bf16[32,2048]{1,0:T(8,128)(2,1)S(1)}, bf16[32,2048]{1,0:T(8,128)(2,1)S(1)}, u32[]{:S(2)}, u32[]{:S(2)}) collective-permute-start(bf16[32,2048]{1,0:T(8,128)(2,1)S(1)} %get-tuple-element.17), channel_id=1, source_target_pairs={{0,12},{4,16},{8,20},{12,24},{16,28},{20,0},{24,4},{28,8},{1,13},{... | collective-permute-start | bytes 393224 | tf_op jit(solution)/shard_map/ppermute | solution.py:187
  30.2 9.1 %collective-permute-start.13 = (bf16[32,2048]{1,0:T(8,128)(2,1)S(1)}, bf16[32,2048]{1,0:T(8,128)(2,1)S(1)}, u32[]{:S(2)}, u32[]{:S(2)}) collective-permute-start(bf16[32,2048]{1,0:T(8,128)(2,1)S(1)} %get-tuple-element.16), channel_id=1, source_target_pairs={{0,16},{4,20},{8,24},{12,28},{16,0},{20,4},{24,8},{28,12},{1,17},{... | collective-permute-start | bytes 393224 | tf_op jit(solution)/shard_map/ppermute | solution.py:187
  34.1 10.6 %collective-permute-start.14 = (bf16[32,2048]{1,0:T(8,128)(2,1)S(1)}, bf16[32,2048]{1,0:T(8,128)(2,1)S(1)}, u32[]{:S(2)}, u32[]{:S(2)}) collective-permute-start(bf16[32,2048]{1,0:T(8,128)(2,1)S(1)} %get-tuple-element.15), channel_id=1, source_target_pairs={{0,20},{4,24},{8,28},{12,0},{16,4},{20,8},{24,12},{28,16},{1,21},{... | collective-permute-start | bytes 393224 | tf_op jit(solution)/shard_map/ppermute | solution.py:187
  39.2 10.0 %collective-permute-start.15 = (bf16[32,2048]{1,0:T(8,128)(2,1)S(1)}, bf16[32,2048]{1,0:T(8,128)(2,1)S(1)}, u32[]{:S(2)}, u32[]{:S(2)}) collective-permute-start(bf16[32,2048]{1,0:T(8,128)(2,1)S(1)} %get-tuple-element.14), channel_id=1, source_target_pairs={{0,24},{4,28},{8,0},{12,4},{16,8},{20,12},{24,16},{28,20},{1,25},{... | collective-permute-start | bytes 393224 | tf_op jit(solution)/shard_map/ppermute | solution.py:187
  44.7 6.9 %collective-permute-start.16 = (bf16[32,2048]{1,0:T(8,128)(2,1)S(1)}, bf16[32,2048]{1,0:T(8,128)(2,1)S(1)}, u32[]{:S(2)}, u32[]{:S(2)}) collective-permute-start(bf16[32,2048]{1,0:T(8,128)(2,1)S(1)} %get-tuple-element.13), channel_id=1, source_target_pairs={{0,28},{4,0},{8,4},{12,8},{16,12},{20,16},{24,20},{28,24},{1,29},{... | collective-permute-start | bytes 393224 | tf_op jit(solution)/shard_map/ppermute | solution.py:187
  52.3 2.9 %copy-start.6 = (bf16[512,2048]{1,0:T(8,128)(2,1)}, bf16[512,2048]{1,0:T(8,128)(2,1)S(1)}, u32[]{:S(2)}) copy-start(bf16[512,2048]{1,0:T(8,128)(2,1)S(1)} %get-tuple-element.29) | copy-start | bytes 6291460
  52.3 3.0 %copy-start.11 = (f32[256,2]{0,1:T(2,128)S(1)}, f32[256,2]{0,1:T(2,128)}, u32[]{:S(2)}) copy-start(f32[256,2]{0,1:T(2,128)} %param.26) | copy-start | bytes 6148
  52.3 29.0 %collective-permute-start.19 = (bf16[256,2048]{1,0:T(8,128)(2,1)}, bf16[256,2048]{1,0:T(8,128)(2,1)}, u32[]{:S(2)}, u32[]{:S(2)}) collective-permute-start(bf16[256,2048]{1,0:T(8,128)(2,1)} %get-tuple-element.30), channel_id=1, source_target_pairs={{0,2},{1,3},{2,0},{3,1},{4,6},{5,7},{6,4},{7,5},{8,10},{9,11},{10,... | collective-permute-start | bytes 3145736 | tf_op jit(solution)/shard_map/ppermute | solution.py:31
  55.2 27.5 %collective-permute-start.17 = (bf16[256,2048]{1,0:T(8,128)(2,1)}, bf16[256,2048]{1,0:T(8,128)(2,1)S(1)}, u32[]{:S(2)}, u32[]{:S(2)}) collective-permute-start(bf16[256,2048]{1,0:T(8,128)(2,1)} %get-tuple-element.30), channel_id=1, source_target_pairs={{0,1},{1,0},{2,3},{3,2},{4,5},{5,4},{6,7},{7,6},{8,9},{9,8},{10,11... | collective-permute-start | bytes 3145736 | tf_op jit(solution)/shard_map/ppermute | solution.py:31
  55.3 27.4 %copy-start.7 = (bf16[512,2048]{1,0:T(8,128)(2,1)S(1)}, bf16[512,2048]{1,0:T(8,128)(2,1)}, u32[]{:S(2)}) copy-start(bf16[512,2048]{1,0:T(8,128)(2,1)} %copy-done.6) | copy-start | bytes 6291460
  55.3 10.7 %collective-permute-start.3 = (bf16[1,512,128]{2,1,0:T(8,128)(2,1)}, bf16[1,512,128]{2,1,0:T(8,128)(2,1)S(1)}, u32[]{:S(2)}, u32[]{:S(2)}) collective-permute-start(bf16[1,512,128]{2,1,0:T(8,128)(2,1)} %get-tuple-element.3), channel_id=1, source_target_pairs={{0,16},{4,20},{8,24},{12,28},{1,17},{5,21},{9,25},{13,29},{2,18},{... | collective-permute-start | bytes 393224 | tf_op jit(solution)/shard_map/ppermute | solution.py:130
  58.0 22.0 %collective-permute-start.4 = (bf16[1,512,128]{2,1,0:T(8,128)(2,1)}, bf16[1,512,128]{2,1,0:T(8,128)(2,1)S(1)}, u32[]{:S(2)}, u32[]{:S(2)}) collective-permute-start(bf16[1,512,128]{2,1,0:T(8,128)(2,1)} %get-tuple-element.3), channel_id=1, source_target_pairs={{0,20},{4,24},{8,28},{1,21},{5,25},{9,29},{2,22},{6,26},{10,30},{3... | collective-permute-start | bytes 393224 | tf_op jit(solution)/shard_map/ppermute | solution.py:130
  63.6 17.1 %collective-permute-start.5 = (bf16[1,512,128]{2,1,0:T(8,128)(2,1)}, bf16[1,512,128]{2,1,0:T(8,128)(2,1)S(1)}, u32[]{:S(2)}, u32[]{:S(2)}) collective-permute-start(bf16[1,512,128]{2,1,0:T(8,128)(2,1)} %get-tuple-element.3), channel_id=1, source_target_pairs={{0,24},{4,28},{1,25},{5,29},{2,26},{6,30},{3,27},{7,31}} | collective-permute-start | bytes 393224 | tf_op jit(solution)/shard_map/ppermute | solution.py:130
  66.1 52.5 %collective-permute-start.6 = (bf16[1,512,128]{2,1,0:T(8,128)(2,1)}, bf16[1,512,128]{2,1,0:T(8,128)(2,1)S(1)}, u32[]{:S(2)}, u32[]{:S(2)}) collective-permute-start(bf16[1,512,128]{2,1,0:T(8,128)(2,1)} %get-tuple-element.3), channel_id=1, source_target_pairs={{0,28},{1,29},{2,30},{3,31}} | collective-permute-start | bytes 393224 | tf_op jit(solution)/shard_map/ppermute | solution.py:130
  81.3 2.4 %copy-start.12 = (bf16[1,2048,896]{2,1,0:T(8,128)(2,1)S(1)}, bf16[1,2048,896]{2,1,0:T(8,128)(2,1)}, u32[]{:S(2)}) copy-start(bf16[1,2048,896]{2,1,0:T(8,128)(2,1)} %param.29) | copy-start | bytes 11010052
  81.3 5.9 %collective-permute-start.20 = (bf16[256,2048]{1,0:T(8,128)(2,1)}, bf16[256,2048]{1,0:T(8,128)(2,1)S(1)}, u32[]{:S(2)}, u32[]{:S(2)}) collective-permute-start(bf16[256,2048]{1,0:T(8,128)(2,1)} %collective-permute-done.19), channel_id=1, source_target_pairs={{0,1},{1,0},{2,3},{3,2},{4,5},{5,4},{6,7},{7,6},{8,9},{9,8},{10,11... | collective-permute-start | bytes 3145736 | tf_op jit(solution)/shard_map/ppermute | solution.py:31
  83.7 3.6 %copy-start.8 = (bf16[512,2048]{1,0:T(8,128)(2,1)}, bf16[512,2048]{1,0:T(8,128)(2,1)S(1)}, u32[]{:S(2)}) copy-start(bf16[512,2048]{1,0:T(8,128)(2,1)S(1)} %constant_dynamic-update-slice_fusion.15) | copy-start | bytes 6291460
  87.3 1.3 copy-start.3
  102.4 13.1 %collective-permute-start.21 = (bf16[256,2048]{1,0:T(8,128)(2,1)}, bf16[256,2048]{1,0:T(8,128)(2,1)}, u32[]{:S(2)}, u32[]{:S(2)}) collective-permute-start(bf16[256,2048]{1,0:T(8,128)(2,1)} %slice.91), channel_id=1, source_target_pairs={{0,1},{1,0},{2,3},{3,2},{4,5},{5,4},{6,7},{7,6},{8,9},{9,8},{10,11... | collective-permute-start | bytes 3145736 | tf_op jit(solution)/shard_map/ppermute | solution.py:31
  114.9 11.9 %copy-start.10 = (s32[8]{0:T(128)S(1)}, s32[8]{0:T(128)}, u32[]{:S(2)}) copy-start(s32[8]{0:T(128)} %copy-done.9) | copy-start | bytes 100
  114.9 33.8 %collective-permute-start.18 = (bf16[256,2048]{1,0:T(8,128)(2,1)}, bf16[256,2048]{1,0:T(8,128)(2,1)}, u32[]{:S(2)}, u32[]{:S(2)}) collective-permute-start(bf16[256,2048]{1,0:T(8,128)(2,1)} %slice.89), channel_id=1, source_target_pairs={{0,1},{1,0},{2,3},{3,2},{4,5},{5,4},{6,7},{7,6},{8,9},{9,8},{10,11... | collective-permute-start | bytes 3145736 | tf_op jit(solution)/shard_map/ppermute | solution.py:31
  118.0 30.7 %collective-permute-start.22 = (bf16[256,2048]{1,0:T(8,128)(2,1)}, bf16[256,2048]{1,0:T(8,128)(2,1)S(1)}, u32[]{:S(2)}, u32[]{:S(2)}) collective-permute-start(bf16[256,2048]{1,0:T(8,128)(2,1)} %add_convert_fusion.1), channel_id=1, source_target_pairs={{0,2},{1,3},{2,0},{3,1},{4,6},{5,7},{6,4},{7,5},{8,10},{9,11},{10,... | collective-permute-start | bytes 3145736 | tf_op jit(solution)/shard_map/ppermute | solution.py:31
  124.6 20.9 %collective-permute-start.8 = (bf16[128,256]{1,0:T(8,128)(2,1)S(1)}, bf16[128,256]{1,0:T(8,128)(2,1)S(1)}, u32[]{:S(2)}, u32[]{:S(2)}) collective-permute-start(bf16[128,256]{1,0:T(8,128)(2,1)S(1)} %get-tuple-element.27), channel_id=1, source_target_pairs={{0,2},{1,3},{2,0},{3,1},{4,6},{5,7},{6,4},{7,5},{8,10},{9,11},{10,... | collective-permute-start | bytes 196616 | tf_op jit(solution)/shard_map/ppermute | solution.py:31
  126.1 19.3 %collective-permute-start.9 = (bf16[128,256]{1,0:T(8,128)(2,1)S(1)}, bf16[128,256]{1,0:T(8,128)(2,1)S(1)}, u32[]{:S(2)}, u32[]{:S(2)}) collective-permute-start(bf16[128,256]{1,0:T(8,128)(2,1)S(1)} %get-tuple-element.26), channel_id=1, source_target_pairs={{0,3},{1,2},{2,1},{3,0},{4,7},{5,6},{6,5},{7,4},{8,11},{9,10},{10,... | collective-permute-start | bytes 196616 | tf_op jit(solution)/shard_map/ppermute | solution.py:31
  126.1 19.3 %collective-permute-start.7 = (bf16[128,256]{1,0:T(8,128)(2,1)S(1)}, bf16[128,256]{1,0:T(8,128)(2,1)S(1)}, u32[]{:S(2)}, u32[]{:S(2)}) collective-permute-start(bf16[128,256]{1,0:T(8,128)(2,1)S(1)} %get-tuple-element.28), channel_id=1, source_target_pairs={{0,1},{1,0},{2,3},{3,2},{4,5},{5,4},{6,7},{7,6},{8,9},{9,8},{10,11... | collective-permute-start | bytes 196616 | tf_op jit(solution)/shard_map/ppermute | solution.py:31
  145.5 3.2 %copy-start.2 = (bf16[512,2048]{1,0:T(8,128)(2,1)S(1)}, bf16[512,2048]{1,0:T(8,128)(2,1)}, u32[]{:S(2)}) copy-start(bf16[512,2048]{1,0:T(8,128)(2,1)} %fusion.15) | copy-start | bytes 6291460
  150.5 8.2 %copy-start.4 = (f32[2048]{0:T(1024)S(1)}, f32[2048]{0:T(1024)}, u32[]{:S(2)}) copy-start(f32[2048]{0:T(1024)} %param.23) | copy-start | bytes 24580
  150.6 12.5 %collective-permute-start.23 = (bf16[32,2048]{1,0:T(8,128)(2,1)S(1)}, bf16[32,2048]{1,0:T(8,128)(2,1)S(1)}, u32[]{:S(2)}, u32[]{:S(2)}) collective-permute-start(bf16[32,2048]{1,0:T(8,128)(2,1)S(1)} %get-tuple-element.10), channel_id=1, source_target_pairs={{0,28},{4,0},{8,4},{12,8},{16,12},{20,16},{24,20},{28,24},{1,29},{... | collective-permute-start | bytes 393224 | tf_op jit(solution)/shard_map/ppermute | solution.py:187
  159.6 5.8 %collective-permute-start.24 = (bf16[32,2048]{1,0:T(8,128)(2,1)S(1)}, bf16[32,2048]{1,0:T(8,128)(2,1)S(1)}, u32[]{:S(2)}, u32[]{:S(2)}) collective-permute-start(bf16[32,2048]{1,0:T(8,128)(2,1)S(1)} %get-tuple-element.9), channel_id=1, source_target_pairs={{0,24},{4,28},{8,0},{12,4},{16,8},{20,12},{24,16},{28,20},{1,25},{... | collective-permute-start | bytes 393224 | tf_op jit(solution)/shard_map/ppermute | solution.py:187
  159.6 8.6 %collective-permute-start.25 = (bf16[32,2048]{1,0:T(8,128)(2,1)S(1)}, bf16[32,2048]{1,0:T(8,128)(2,1)S(1)}, u32[]{:S(2)}, u32[]{:S(2)}) collective-permute-start(bf16[32,2048]{1,0:T(8,128)(2,1)S(1)} %get-tuple-element.8), channel_id=1, source_target_pairs={{0,20},{4,24},{8,28},{12,0},{16,4},{20,8},{24,12},{28,16},{1,21},{... | collective-permute-start | bytes 393224 | tf_op jit(solution)/shard_map/ppermute | solution.py:187
  159.6 17.7 %collective-permute-start.26 = (bf16[32,2048]{1,0:T(8,128)(2,1)S(1)}, bf16[32,2048]{1,0:T(8,128)(2,1)S(1)}, u32[]{:S(2)}, u32[]{:S(2)}) collective-permute-start(bf16[32,2048]{1,0:T(8,128)(2,1)S(1)} %get-tuple-element.7), channel_id=1, source_target_pairs={{0,16},{4,20},{8,24},{12,28},{16,0},{20,4},{24,8},{28,12},{1,17},{... | collective-permute-start | bytes 393224 | tf_op jit(solution)/shard_map/ppermute | solution.py:187
  163.1 20.5 %collective-permute-start.27 = (bf16[32,2048]{1,0:T(8,128)(2,1)S(1)}, bf16[32,2048]{1,0:T(8,128)(2,1)S(1)}, u32[]{:S(2)}, u32[]{:S(2)}) collective-permute-start(bf16[32,2048]{1,0:T(8,128)(2,1)S(1)} %get-tuple-element.6), channel_id=1, source_target_pairs={{0,12},{4,16},{8,20},{12,24},{16,28},{20,0},{24,4},{28,8},{1,13},{... | collective-permute-start | bytes 393224 | tf_op jit(solution)/shard_map/ppermute | solution.py:187
  163.1 20.5 %collective-permute-start.28 = (bf16[32,2048]{1,0:T(8,128)(2,1)S(1)}, bf16[32,2048]{1,0:T(8,128)(2,1)S(1)}, u32[]{:S(2)}, u32[]{:S(2)}) collective-permute-start(bf16[32,2048]{1,0:T(8,128)(2,1)S(1)} %get-tuple-element.5), channel_id=1, source_target_pairs={{0,8},{4,12},{8,16},{12,20},{16,24},{20,28},{24,0},{28,4},{1,9},{5... | collective-permute-start | bytes 393224 | tf_op jit(solution)/shard_map/ppermute | solution.py:187
  165.4 18.2 %collective-permute-start.29 = (bf16[32,2048]{1,0:T(8,128)(2,1)S(1)}, bf16[32,2048]{1,0:T(8,128)(2,1)S(1)}, u32[]{:S(2)}, u32[]{:S(2)}) collective-permute-start(bf16[32,2048]{1,0:T(8,128)(2,1)S(1)} %get-tuple-element.4), channel_id=1, source_target_pairs={{0,4},{4,8},{8,12},{12,16},{16,20},{20,24},{24,28},{28,0},{1,5},{5... | collective-permute-start | bytes 393224 | tf_op jit(solution)/shard_map/ppermute | solution.py:187
  183.6 0.8 copy-start.5
